TPU v7x, 32 devices: a whole 2x2x4 slice. The times are simulated.
32 devices in a mesh: ep: 8 (over z, core), tp: 4 (over y, x).
Axes of the slice: x: 2, y: 2, z: 4, core: 2. Of those that a mesh axis runs over, the one named last changes fastest.
Arguments:
- tokens: bfloat16 [1536, 4096], P('ep'), may hold values from -6 to 6
- expert_ids: int32 [1536, 2], P('ep'), may hold values from 0 to 7, all different within a row; in each aligned block of 192 rows (0 to 191, 192 to 383, ...) at most 60 rows name the same one
- route_weight: float32 [1536, 2], P('ep'), may hold values from 0.1 to 1
- norm_gain: float32 [4096], replicated, may hold values from 0.1 to 1.9
- gate_weight: bfloat16 [8, 4096, 4096], P('ep', None, 'tp'), may hold values from -0.28125 to 0.28125
- up_weight: bfloat16 [8, 4096, 4096], P('ep', None, 'tp'), may hold values from -0.28125 to 0.28125
- down_weight: bfloat16 [8, 4096, 4096], P('ep', None, 'tp'), may hold values from -0.028076172 to 0.028076172
Outputs:
- mixed: bfloat16 [1536, 4096], P('ep', 'tp')
Inputs may be any that keep to these rules, and one draw needn't show every extreme that they name: `expert_ids`: each row names 2 different experts. In each aligned block of 192 rows (the tokens of one index of ep) no expert is named by more than 60 rows, and in some block some expert is named by exactly 60 rows.
All inputs are finite; a program needn't handle non-finite values.
Results may differ from a plain program's by a relative error of at most 0.007.
Values may be sent and summed in bfloat16 or wider, within the bound.
A program may use at most 64 MiB of HBM per device.

v0:
```python
import jax
import jax.numpy as jnp
from jax import lax
from jax.sharding import PartitionSpec as P

EPS = 1e-06
LIMIT = 7.0
ALPHA = 1.702


def rms_norm(tokens, norm_gain):
    values = tokens.astype(jnp.float32)
    scale = lax.rsqrt(jnp.mean(values * values, axis=-1, keepdims=True) + EPS)
    return (values * scale * norm_gain).astype(jnp.bfloat16)


def clamped_unit(gate_pre, up_pre):
    gate = jnp.minimum(gate_pre, LIMIT)
    up_part = jnp.clip(up_pre, -LIMIT, LIMIT)
    return ((up_part + 1.0) * gate * jax.nn.sigmoid(ALPHA * gate)).astype(jnp.bfloat16)


def slot_numbers(id_blocks, experts, capacity):
    onehot = (id_blocks[:, :, None] == jnp.arange(experts, dtype=jnp.int32)[None, None, :]).astype(
        jnp.int32
    )
    before = jnp.cumsum(onehot, axis=1) - onehot
    position = jnp.sum(before * onehot, axis=2)
    return id_blocks * capacity + position


def project_down(hidden, down_weight):
    result = jnp.einsum(
        "sejf,efd->sejd",
        lax.all_gather(hidden, "tp", axis=3, tiled=True),
        down_weight,
        preferred_element_type=jnp.float32,
    )
    return result.astype(jnp.bfloat16)


def on_device(tokens, expert_ids, route_weight, norm_gain, gate_weight, up_weight, down_weight):
    n_ep = lax.axis_size("ep")
    n_tp = lax.axis_size("tp")
    tok_rows, width = tokens.shape
    top = expert_ids.shape[1]
    local_experts = gate_weight.shape[0]
    experts = local_experts * n_ep
    capacity = 5 * tok_rows * top // (4 * experts)
    cols = width // n_tp
    normed = rms_norm(tokens, norm_gain)
    dest = slot_numbers(expert_ids.reshape(1, tok_rows * top), experts, capacity).reshape(-1)
    slot_range = jnp.arange(experts * capacity, dtype=jnp.int32)
    match = slot_range[:, None] == dest[None, :]
    pick = jnp.any(match.reshape(experts * capacity, tok_rows, top), axis=2).astype(jnp.bfloat16)
    own = lax.dynamic_slice_in_dim(normed, lax.axis_index("tp") * cols, cols, 1)
    buffer = jnp.dot(pick, own, preferred_element_type=jnp.float32).astype(jnp.bfloat16)
    buffer = buffer.reshape(n_ep, local_experts, capacity, cols)
    arrived = lax.all_to_all(buffer, "ep", split_axis=0, concat_axis=0, tiled=True)
    piece = lax.all_gather(arrived, "tp", axis=3, tiled=True)
    gate_part = jnp.einsum("sejd,edf->sejf", piece, gate_weight, preferred_element_type=jnp.float32)
    up_part = jnp.einsum("sejd,edf->sejf", piece, up_weight, preferred_element_type=jnp.float32)
    hidden = clamped_unit(gate_part, up_part)
    result = project_down(hidden, down_weight)
    back = lax.all_to_all(result, "ep", split_axis=0, concat_axis=0, tiled=True).reshape(
        experts * capacity, cols
    )
    chosen = jnp.transpose(match).astype(jnp.bfloat16)
    per_copy = jnp.dot(chosen, back, preferred_element_type=jnp.float32).reshape(
        tok_rows, top, cols
    )
    mixed = jnp.sum(per_copy * route_weight[:, :, None], axis=1)
    return mixed.astype(jnp.bfloat16)


def solution(mesh):
    placed = (
        P("ep", None),
        P("ep", None),
        P("ep", None),
        P(),
        P("ep", None, "tp"),
        P("ep", None, "tp"),
        P("ep", None, "tp"),
    )
    return jax.shard_map(
        on_device, mesh=mesh, in_specs=placed, out_specs=P("ep", "tp"), check_vma=False
    )
```

profile of v0, /device:TPU:0, one launch (start us, length us, event | category | flops | bytes accessed | tf_op | source)
XLA Modules:
  0.0 220.5 jit_solution(3522461065963199480)
XLA Ops:
  6.5 0.0 copy-start
  6.5 0.0 all-gather.3.cloned.1.call-start
  6.5 0.0 copy-start.1
  6.5 3.5 %convert_element_type.41 = f32[192,4096]{1,0:T(8,128)} convert(bf16[192,4096]{1,0:T(8,128)(2,1)} %param.7) | non-fusion elementwise | flops 786432 | bytes 4718592 | tf_op jit(solution)/shard_map/convert_element_type | solution.py:12
  10.1 0.0 copy-done
  10.1 0.4 multiply_reduce_fusion
  10.5 0.0 copy-done.1
  10.5 0.1 copy.28
  10.6 0.1 reshape.211
  10.8 0.9 reduce-window.6
  11.6 0.2 slice_reduce_fusion
  11.9 0.1 fusion.36
  12.0 0.1 reduce_sum.30
  12.1 0.1 copy.29
  12.2 0.2 fusion.30
  12.4 0.7 dynamic-slice
  13.1 1.6 convolution_convert_fusion
  14.8 0.2 reshape.217
  14.9 32.8 %all_to_all.10 = bf16[8,1,60,1024]{3,2,1,0:T(8,128)(2,1)} all-to-all(bf16[8,1,60,1024]{3,2,1,0:T(8,128)(2,1)S(1)} %bitcast.73), channel_id=1, replica_groups=mesh['ep'=8,'tp'=4] {'ep'}, dimensions={0} | all-to-all | bytes 1966080 | tf_op jit(solution)/shard_map/all_to_all | solution.py:59
  47.8 0.0 all-gather.3.cloned.1.call-update
  47.8 0.0 all-gather.5.cloned.1.call-start
  47.8 51.6 %all-gather.3.cloned.1.call-done = bf16[8,1,60,4096]{3,2,0,1:T(8,128)(2,1)} async-done(((bf16[8,1,60,1024]{3,2,0,1:T(8,128)(2,1)}), bf16[8,1,60,4096]{3,2,0,1:T(8,128)(2,1)}) %all-gather.3.cloned.1.call-update) | async-done | bytes 3932176 | tf_op jit(solution)/shard_map/all_gather | solution.py:60
  99.4 0.0 copy-start.2
  99.4 9.1 %fusion.2 = f32[8,60,1024]{2,1,0:T(8,128)S(1)} fusion(bf16[1,4096,1024]{2,1,0:T(8,128)(2,1)} %param.11, bf16[8,1,60,4096]{3,2,0,1:T(8,128)(2,1)} %all-gather.3.cloned.1.call-done), kind=kOutput, calls=%fused_computation.2 | convolution fusion | flops 4026531840 | bytes 14286848 | tf_op jit(solution)/shard_map/sejd,edf->sejf/dot_general | solution.py:61
  108.6 0.0 copy-done.2
  108.6 9.4 %fusion.23 = bf16[8,1,60,1024]{3,2,0,1:T(8,128)(2,1)} fusion(f32[8,60,1024]{2,1,0:T(8,128)S(1)} %fusion.2, bf16[1,4096,1024]{2,1,0:T(8,128)(2,1)} %param.12, bf16[8,1,60,4096]{3,2,0,1:T(8,128)(2,1)S(1)} %copy-done.2), kind=kOutput, calls=%fused_computation.15 | convolution fusion | flops 4031447040 | bytes 15269888 | tf_op jit(solution)/shard_map/sejd,edf->sejf/dot_general | solution.py:62
  118.0 0.0 all-gather.5.cloned.1.call-update
  118.0 52.7 %all-gather.5.cloned.1.call-done = bf16[8,1,60,4096]{3,2,0,1:T(8,128)(2,1)} async-done(((bf16[8,1,60,1024]{3,2,0,1:T(8,128)(2,1)}), bf16[8,1,60,4096]{3,2,0,1:T(8,128)(2,1)}) %all-gather.5.cloned.1.call-update) | async-done | bytes 3932176 | tf_op jit(solution)/shard_map/all_gather | solution.py:35
  170.7 10.1 %fusion.18 = bf16[8,1,60,1024]{3,2,1,0:T(8,128)(2,1)} fusion(bf16[1,4096,1024]{2,1,0:T(8,128)(2,1)} %param.13, bf16[8,1,60,4096]{3,2,0,1:T(8,128)(2,1)} %all-gather.5.cloned.1.call-done), kind=kOutput, calls=%fused_computation.14 | convolution fusion | flops 4027023360 | bytes 13303808 | tf_op jit(solution)/shard_map/sejf,efd->sejd/dot_general | solution.py:33
  180.8 0.0 copy-start.3
  180.8 4.7 %all-to-all-start.1 = ((bf16[8,1,60,1024]{3,2,1,0:T(8,128)(2,1)}), bf16[8,1,60,1024]{3,2,1,0:T(8,128)(2,1)S(1)}, u32[]{:S(2)}, u32[]{:S(2)}) async-start(bf16[8,1,60,1024]{3,2,1,0:T(8,128)(2,1)} %fusion.18), calls=%async_computation.1 | async-start | bytes 2097152 | tf_op jit(solution)/shard_map/all_to_all | solution.py:65
  185.6 0.2 iota_compare_fusion.1
  185.8 0.3 eq.60
  186.0 26.1 %all-to-all-done.1 = bf16[8,1,60,1024]{3,2,1,0:T(8,128)(2,1)S(1)} async-done(((bf16[8,1,60,1024]{3,2,1,0:T(8,128)(2,1)}), bf16[8,1,60,1024]{3,2,1,0:T(8,128)(2,1)S(1)}, u32[]{:S(2)}, u32[]{:S(2)}) %all-to-all-start.1) | async-done | bytes 983072 | tf_op jit(solution)/shard_map/all_to_all | solution.py:65
  212.1 0.2 reshape.235
  212.3 0.0 copy-done.3
  212.3 1.4 multiply_reduce_fusion.1
  (8 shorter events, 0.0 us)
Async XLA Ops:
  6.5 3.6 %copy-start = (bf16[192,4096]{1,0:T(8,128)(2,1)S(1)}, bf16[192,4096]{1,0:T(8,128)(2,1)}, u32[]{:S(2)}) copy-start(bf16[192,4096]{1,0:T(8,128)(2,1)} %param.7) | copy-start | bytes 4718596
  6.5 92.9 %all-gather.3.cloned.1.call-start = ((), (), s32[]{:S(2)}) async-start(), calls=%async_computation.2 | async-start | bytes 5242880 | tf_op jit(solution)/shard_map/all_gather | solution.py:60
  6.5 4.0 %copy-start.1 = (s32[192,2]{0,1:T(2,128)S(1)}, s32[192,2]{0,1:T(2,128)}, u32[]{:S(2)}) copy-start(s32[192,2]{0,1:T(2,128)} %param.8) | copy-start | bytes 4612
  47.8 122.9 %all-gather.5.cloned.1.call-start = ((), (), s32[]{:S(2)}) async-start(), calls=%async_computation.3 | async-start | bytes 5242880 | tf_op jit(solution)/shard_map/all_gather | solution.py:35
  99.4 9.1 %copy-start.2 = (bf16[8,1,60,4096]{3,2,0,1:T(8,128)(2,1)S(1)}, bf16[8,1,60,4096]{3,2,0,1:T(8,128)(2,1)}, u32[]{:S(2)}) copy-start(bf16[8,1,60,4096]{3,2,0,1:T(8,128)(2,1)} %all-gather.3.cloned.1.call-done) | copy-start | bytes 11796484
  180.8 31.5 %copy-start.3 = (f32[192,2]{0,1:T(2,128)S(1)}, f32[192,2]{0,1:T(2,128)}, u32[]{:S(2)}) copy-start(f32[192,2]{0,1:T(2,128)} %param.9) | copy-start | bytes 4612
  180.8 31.3 %all-to-all-start.1 = ((bf16[8,1,60,1024]{3,2,1,0:T(8,128)(2,1)}), bf16[8,1,60,1024]{3,2,1,0:T(8,128)(2,1)S(1)}, u32[]{:S(2)}, u32[]{:S(2)}) async-start(bf16[8,1,60,1024]{3,2,1,0:T(8,128)(2,1)} %fusion.18), calls=%async_computation.1 | async-start | bytes 2097152 | tf_op jit(solution)/shard_map/all_to_all | solution.py:65
Sparse Core Ops, SparseCore 0:
  47.9 51.4 all-gather.2
  118.1 52.5 all-gather.4
where the time goes:
time: 221 us
  waiting for transfers between devices  130 us (59%)
  blocking collectives  32.8 us (15%)
  matrix products  31.6 us (14%)
  between operations  13.5 us (6%)
  other arithmetic  5.26 us (2%)
  starting transfers between devices  4.78 us (2%)
    all_gather x1, waiting for transfers between devices, project_down(): lax.all_gather(hidden, 'tp', axis=3, tiled=True)  52.7 us
    all_gather x1, waiting for transfers between devices, on_device(): piece = lax.all_gather(arrived, 'tp', axis=3, tiled=True)  51.6 us
    all_to_all x1, blocking collectives, on_device(): lax.all_to_all(buffer, 'ep', split_axis=0, concat_axis=0, tiled=True)  32.8 us
    all_to_all x1, waiting for transfers between devices, on_device(): lax.all_to_all(result, 'ep', split_axis=0, concat_axis=0, tiled=True)  26.1 us
    dot_general x1, matrix products, project_down(): jnp.einsum('sejf,efd->sejd', lax.all_gather(hidden, 'tp', axis=3, tiled=T...  10.1 us
    dot_general x1, matrix products, on_device(): jnp.einsum('sejd,edf->sejf', piece, up_weight, preferred_element_type=jnp...  9.37 us
    dot_general x1, matrix products, on_device(): jnp.einsum('sejd,edf->sejf', piece, gate_weight, preferred_element_type=j...  9.13 us
    all_to_all x1, starting transfers between devices, on_device(): lax.all_to_all(result, 'ep', split_axis=0, concat_axis=0, tiled=True)  4.74 us
  transfers between devices with their start and end apart: 3, of which 3 were waited for; matrix products, arithmetic and copies ran while one was open for 0% of the time, Pallas kernels for 0%

commit v1 on v0

--- a/solution.py
+++ b/solution.py
@@ -30,12 +30,38 @@
 
 
 def project_down(hidden, down_weight):
-    result = jnp.einsum(
+    peers, index, width_2 = (lax.axis_size("tp"), lax.axis_index("tp"), hidden.shape[3])
+    upward = [(i, (i + 1) % peers) for i in range(peers)]
+    backward = [(i, (i - 1) % peers) for i in range(peers)]
+    middle = peers // 2
+    from_left = from_right = hidden
+    running = jnp.einsum(
         "sejf,efd->sejd",
-        lax.all_gather(hidden, "tp", axis=3, tiled=True),
-        down_weight,
+        hidden,
+        lax.dynamic_slice_in_dim(down_weight, index * width_2, hidden.shape[3], axis=1),
         preferred_element_type=jnp.float32,
     )
+    for hop in range(1, middle + 1):
+        from_left = lax.ppermute(from_left, "tp", upward)
+        if hop < peers - middle:
+            from_right = lax.ppermute(from_right, "tp", backward)
+            running = running + jnp.einsum(
+                "sejf,efd->sejd",
+                from_right,
+                lax.dynamic_slice_in_dim(
+                    down_weight, (index + hop) % peers * width_2, from_right.shape[3], axis=1
+                ),
+                preferred_element_type=jnp.float32,
+            )
+        running = running + jnp.einsum(
+            "sejf,efd->sejd",
+            from_left,
+            lax.dynamic_slice_in_dim(
+                down_weight, (index - hop) % peers * width_2, from_left.shape[3], axis=1
+            ),
+            preferred_element_type=jnp.float32,
+        )
+    result = running
     return result.astype(jnp.bfloat16)
 
 

time: 221 us -> 226 us (1.023)
  starting transfers between devices: 4.78 us -> 8.29 us
    ppermute x0 -> x3, waiting for transfers between devices: none -> 54.1 us  [the longest x2 39.7 us: project_down(): from_left = lax.ppermute(from_left, 'tp', upward)]
    all_gather x1 -> x0, waiting for transfers between devices: 52.7 us -> none  [project_down(): lax.all_gather(hidden, 'tp', axis=3, tiled=True)]
    ppermute x0 -> x3, starting transfers between devices: none -> 3.55 us  [the longest x2 2.09 us: project_down(): from_left = lax.ppermute(from_left, 'tp', upward)]
    dot_general x1 -> x4, matrix products: 10.1 us -> 11.1 us  [the longest x2 5.52 us: project_down(): jnp.einsum('sejf,efd->sejd', from_left, lax.dynamic_slice_in_dim(down_wei...]
  transfers between devices with their start and end apart: 3 -> 5, of which waited for: 3 -> 5; matrix products, arithmetic and copies ran while one was open for 0% -> 4% of each run, Pallas kernels for 0% -> 0%
where the time goes in v1:
time: 226 us; the launch traced here: 225 us
  waiting for transfers between devices  132 us (58%)
  blocking collectives  32.8 us (15%)
  matrix products  31.4 us (14%)
  between operations  13.6 us (6%)
  starting transfers between devices  8.29 us (4%)
  local copies, waits for them, and re-layouts  3.75 us (2%)
  other arithmetic  3.58 us (2%)
    all_gather x1, waiting for transfers between devices, on_device(): piece = lax.all_gather(arrived, 'tp', axis=3, tiled=True)  51.7 us
    ppermute x2, waiting for transfers between devices, project_down(): from_left = lax.ppermute(from_left, 'tp', upward)  39.7 us
    all_to_all x1, blocking collectives, on_device(): lax.all_to_all(buffer, 'ep', split_axis=0, concat_axis=0, tiled=True)  32.8 us
    all_to_all x1, waiting for transfers between devices, on_device(): lax.all_to_all(result, 'ep', split_axis=0, concat_axis=0, tiled=True)  26.1 us
    ppermute x1, waiting for transfers between devices, project_down(): from_right = lax.ppermute(from_right, 'tp', backward)  14.5 us
    dot_general x1, matrix products, on_device(): jnp.einsum('sejd,edf->sejf', piece, gate_weight, preferred_element_type=j...  9.13 us
    dot_general x1, matrix products, on_device(): jnp.einsum('sejd,edf->sejf', piece, up_weight, preferred_element_type=jnp...  8.38 us
    dot_general x2, matrix products, project_down(): jnp.einsum('sejf,efd->sejd', from_left, lax.dynamic_slice_in_dim(down_wei...  5.52 us
  transfers between devices with their start and end apart: 5, of which 5 were waited for; matrix products, arithmetic and copies ran while one was open for 4% of the time, Pallas kernels for 0%

profile of v1, /device:TPU:0, one launch (start us, length us, event | category | flops | bytes accessed | tf_op | source)
XLA Modules:
  0.0 225.4 jit_solution(4510957676317232278)
XLA Ops:
  6.5 0.0 all-gather.2.cloned.1.call-start
  6.5 0.0 copy-start
  6.5 0.0 copy-start.1
  6.5 1.9 convert_element_type.33
  8.4 0.0 copy-done
  8.4 0.4 multiply_reduce_fusion
  8.8 0.0 copy-done.1
  8.8 0.1 copy.38
  9.0 0.1 reshape.235
  9.1 0.9 reduce-window.6
  10.0 0.2 slice_reduce_fusion
  10.2 0.1 fusion.41
  10.3 0.1 reduce_sum.30
  10.5 0.1 copy.39
  10.6 0.2 fusion.35
  10.7 0.7 dynamic-slice
  11.4 1.5 convolution_convert_fusion
  12.9 1.3 reshape.242
  14.3 32.8 %all_to_all.10 = bf16[8,1,60,1024]{3,2,1,0:T(8,128)(2,1)} all-to-all(bf16[8,1,60,1024]{3,2,1,0:T(8,128)(2,1)S(1)} %bitcast.81), channel_id=1, replica_groups=mesh['ep'=8,'tp'=4] {'ep'}, dimensions={0} | all-to-all | bytes 1966080 | tf_op jit(solution)/shard_map/all_to_all | solution.py:85
  47.1 0.0 all-gather.2.cloned.1.call-update
  47.1 51.7 %all-gather.2.cloned.1.call-done = bf16[8,1,60,4096]{3,2,0,1:T(8,128)(2,1)} async-done(((bf16[8,1,60,1024]{3,2,0,1:T(8,128)(2,1)}), bf16[8,1,60,4096]{3,2,0,1:T(8,128)(2,1)}) %all-gather.2.cloned.1.call-update) | async-done | bytes 3932176 | tf_op jit(solution)/shard_map/all_gather | solution.py:86
  98.8 0.0 copy-start.2
  98.8 9.1 %fusion = f32[8,60,1024]{2,1,0:T(8,128)S(1)} fusion(bf16[1,4096,1024]{2,1,0:T(8,128)(2,1)} %param.11, bf16[8,1,60,4096]{3,2,0,1:T(8,128)(2,1)} %all-gather.2.cloned.1.call-done), kind=kOutput, calls=%fused_computation | convolution fusion | flops 4026531840 | bytes 14286848 | tf_op jit(solution)/shard_map/sejd,edf->sejf/dot_general | solution.py:87
  107.9 0.0 copy-done.2
  107.9 8.4 %multiply_convert_fusion = bf16[8,60,1024]{2,1,0:T(8,128)(2,1)S(1)} fusion(f32[8,60,1024]{2,1,0:T(8,128)S(1)} %fusion, bf16[1,4096,1024]{2,1,0:T(8,128)(2,1)} %param.12, bf16[8,1,60,4096]{3,2,0,1:T(8,128)(2,1)S(1)} %copy-done.2), kind=kOutput, calls=%fused_computation.15 | convolution fusion | flops 4031447040 | bytes 15269888 | tf_op jit(solution)/shard_map/sejd,edf->sejf/dot_general | solution.py:88
  116.3 0.5 copy.42
  116.9 1.5 collective-permute-start.1
  118.4 1.5 collective-permute-start
  119.8 22.6 %collective-permute-done.1 = bf16[8,1,60,1024]{3,0,2,1:T(8,128)(2,1)S(1)} collective-permute-done((bf16[8,1,60,1024]{3,0,2,1:T(8,128)(2,1)S(1)}, bf16[8,1,60,1024]{3,0,2,1:T(8,128)(2,1)S(1)}, u32[]{:S(2)}, u32[]{:S(2)}) %collective-permute-start.1) | collective-permute-done | bytes 983072 | tf_op jit(solution)/shard_map/ppermute | solution.py:45
  142.4 0.6 collective-permute-start.2
  143.0 0.0 slice-start
  143.0 3.0 %fusion.12 = f32[1024,8,60]{0,2,1:T(8,128)S(1)} fusion(bf16[8,60,1024]{2,1,0:T(8,128)(2,1)S(1)} %multiply_convert_fusion, bf16[1,4096,1024]{2,1,0:T(8,128)(2,1)} %param.13, s32[]{:T(128)S(6)} %select_n.28), kind=kOutput, calls=%fused_computation.13 | convolution fusion | flops 1006632960 | bytes 5046276 | tf_op jit(solution)/shard_map/sejf,efd->sejd/dot_general | solution.py:38
  146.0 0.0 slice-start.1
  146.0 3.1 %fusion.8 = f32[1024,8,60]{0,2,1:T(8,128)S(1)} fusion(bf16[1,4096,1024]{2,1,0:T(8,128)(2,1)} %param.13, s32[]{:T(128)S(6)} %select_n.32, bf16[8,1,60,1024]{3,0,2,1:T(8,128)(2,1)S(1)} %collective-permute-done.1), kind=kOutput, calls=%fused_computation.9 | convolution fusion | flops 1006632960 | bytes 5046276 | tf_op jit(solution)/shard_map/sejf,efd->sejd/dot_general | solution.py:56
  149.1 14.5 %collective-permute-done = bf16[8,1,60,1024]{3,0,2,1:T(8,128)(2,1)} collective-permute-done((bf16[8,1,60,1024]{3,0,2,1:T(8,128)(2,1)S(1)}, bf16[8,1,60,1024]{3,0,2,1:T(8,128)(2,1)}, u32[]{:S(2)}, u32[]{:S(2)}) %collective-permute-start) | collective-permute-done | bytes 983072 | tf_op jit(solution)/shard_map/ppermute | solution.py:47
  163.6 0.0 slice-done
  163.6 0.0 slice-done.1
  163.6 2.6 %fusion.10 = f32[1024,8,60]{0,2,1:T(8,128)S(1)} fusion(bf16[1,4096,1024]{2,1,0:T(8,128)(2,1)S(1)} %bitcast.85, s32[]{:T(128)S(6)} %select_n.30, bf16[8,1,60,1024]{3,0,2,1:T(8,128)(2,1)} %collective-permute-done), kind=kOutput, calls=%fused_computation.11 | convolution fusion | flops 1006632960 | bytes 5046276 | tf_op jit(solution)/shard_map/sejf,efd->sejd/dot_general | solution.py:48
  166.2 17.1 %collective-permute-done.2 = bf16[8,1,60,1024]{3,0,2,1:T(8,128)(2,1)S(1)} collective-permute-done((bf16[8,1,60,1024]{3,0,2,1:T(8,128)(2,1)S(1)}, bf16[8,1,60,1024]{3,0,2,1:T(8,128)(2,1)S(1)}, u32[]{:S(2)}, u32[]{:S(2)}) %collective-permute-start.2) | collective-permute-done | bytes 983072 | tf_op jit(solution)/shard_map/ppermute | solution.py:45
  183.3 2.4 %fusion.24 = bf16[8,1,60,1024]{3,2,1,0:T(8,128)(2,1)} fusion(bf16[1,4096,1024]{2,1,0:T(8,128)(2,1)S(1)} %bitcast.85, s32[]{:T(128)S(6)} %select_n.34, f32[1024,8,60]{0,2,1:T(8,128)S(1)} %fusion.8, f32[1024,8,60]{0,2,1:T(8,128)S(1)} %fusion.12, f32[1024,8,60]{0,2,1:T(8,128)S(1)} %fusion.10, bf16[8,1,60,1024]{3,0,2,1:T(8,128)(2,1)S(1)} %collective-permute-done.2), kind=kOutput, calls=%fused_computation.23 | convolution fusion | flops 1008599040 | bytes 10354692 | tf_op jit(solution)/shard_map/sejf,efd->sejd/dot_general | solution.py:56
  185.7 0.0 copy-start.3
  185.7 4.7 %all-to-all-start.1 = ((bf16[8,1,60,1024]{3,2,1,0:T(8,128)(2,1)}), bf16[8,1,60,1024]{3,2,1,0:T(8,128)(2,1)S(1)}, u32[]{:S(2)}, u32[]{:S(2)}) async-start(bf16[8,1,60,1024]{3,2,1,0:T(8,128)(2,1)} %fusion.24), calls=%async_computation.1 | async-start | bytes 2097152 | tf_op jit(solution)/shard_map/all_to_all | solution.py:91
  190.4 0.2 iota_compare_fusion.1
  190.6 0.3 eq.64
  190.9 26.1 %all-to-all-done.1 = bf16[8,1,60,1024]{3,2,1,0:T(8,128)(2,1)S(1)} async-done(((bf16[8,1,60,1024]{3,2,1,0:T(8,128)(2,1)}), bf16[8,1,60,1024]{3,2,1,0:T(8,128)(2,1)S(1)}, u32[]{:S(2)}, u32[]{:S(2)}) %all-to-all-start.1) | async-done | bytes 983072 | tf_op jit(solution)/shard_map/all_to_all | solution.py:91
  217.0 0.2 reshape.268
  217.2 0.0 copy-done.3
  217.2 1.4 multiply_reduce_fusion.1
  (9 shorter events, 0.0 us)
Async XLA Ops:
  6.5 92.2 %all-gather.2.cloned.1.call-start = ((), (), s32[]{:S(2)}) async-start(), calls=%async_computation.2 | async-start | bytes 5242880 | tf_op jit(solution)/shard_map/all_gather | solution.py:86
  6.5 1.9 copy-start
  6.5 2.3 %copy-start.1 = (s32[192,2]{0,1:T(2,128)S(1)}, s32[192,2]{0,1:T(2,128)}, u32[]{:S(2)}) copy-start(s32[192,2]{0,1:T(2,128)} %param.8) | copy-start | bytes 4612
  98.8 9.1 %copy-start.2 = (bf16[8,1,60,4096]{3,2,0,1:T(8,128)(2,1)S(1)}, bf16[8,1,60,4096]{3,2,0,1:T(8,128)(2,1)}, u32[]{:S(2)}) copy-start(bf16[8,1,60,4096]{3,2,0,1:T(8,128)(2,1)} %all-gather.2.cloned.1.call-done) | copy-start | bytes 11796484
  116.9 25.6 %collective-permute-start.1 = (bf16[8,1,60,1024]{3,0,2,1:T(8,128)(2,1)S(1)}, bf16[8,1,60,1024]{3,0,2,1:T(8,128)(2,1)S(1)}, u32[]{:S(2)}, u32[]{:S(2)}) collective-permute-start(bf16[8,1,60,1024]{3,0,2,1:T(8,128)(2,1)S(1)} %copy.42), channel_id=1, source_target_pairs={{0,1},{1,2},{2,3},{3,0},{4,5},{5,6},{6,7},{7,4},{8,9},{9,10},{10,1... | collective-permute-start | bytes 2949128 | tf_op jit(solution)/shard_map/ppermute | solution.py:45
  118.4 45.2 %collective-permute-start = (bf16[8,1,60,1024]{3,0,2,1:T(8,128)(2,1)S(1)}, bf16[8,1,60,1024]{3,0,2,1:T(8,128)(2,1)}, u32[]{:S(2)}, u32[]{:S(2)}) collective-permute-start(bf16[8,1,60,1024]{3,0,2,1:T(8,128)(2,1)S(1)} %copy.42), channel_id=1, source_target_pairs={{0,3},{1,0},{2,1},{3,2},{4,7},{5,4},{6,5},{7,6},{8,11},{9,8},{10,9... | collective-permute-start | bytes 2949128 | tf_op jit(solution)/shard_map/ppermute | solution.py:47
  142.4 40.8 %collective-permute-start.2 = (bf16[8,1,60,1024]{3,0,2,1:T(8,128)(2,1)S(1)}, bf16[8,1,60,1024]{3,0,2,1:T(8,128)(2,1)S(1)}, u32[]{:S(2)}, u32[]{:S(2)}) collective-permute-start(bf16[8,1,60,1024]{3,0,2,1:T(8,128)(2,1)S(1)} %collective-permute-done.1), channel_id=1, source_target_pairs={{0,1},{1,2},{2,3},{3,0},{4,5},{5,6},{6,7},{7,4},{8,9},{9,10},{10,1... | collective-permute-start | bytes 2949128 | tf_op jit(solution)/shard_map/ppermute | solution.py:45
  143.0 20.6 %slice-start = ((s8[8388608]{0:T(1024)(128)(4,1)}), s8[4194304]{0:T(1024)(128)(4,1)S(1)}, s32[]{:S(2)}) async-start(s8[8388608]{0:T(1024)(128)(4,1)} %bitcast.84), calls=%async_computation.3 | async-start | bytes 8388608
  146.0 17.6 %slice-start.1 = ((s8[8388608]{0:T(1024)(128)(4,1)}), s8[4194304]{0:T(1024)(128)(4,1)S(1)}, s32[]{:S(2)}) async-start(s8[8388608]{0:T(1024)(128)(4,1)} %bitcast.84), calls=%async_computation.4 | async-start | bytes 8388608
  185.7 31.5 %copy-start.3 = (f32[192,2]{0,1:T(2,128)S(1)}, f32[192,2]{0,1:T(2,128)}, u32[]{:S(2)}) copy-start(f32[192,2]{0,1:T(2,128)} %param.9) | copy-start | bytes 4612
  185.7 31.3 %all-to-all-start.1 = ((bf16[8,1,60,1024]{3,2,1,0:T(8,128)(2,1)}), bf16[8,1,60,1024]{3,2,1,0:T(8,128)(2,1)S(1)}, u32[]{:S(2)}, u32[]{:S(2)}) async-start(bf16[8,1,60,1024]{3,2,1,0:T(8,128)(2,1)} %fusion.24), calls=%async_computation.1 | async-start | bytes 2097152 | tf_op jit(solution)/shard_map/all_to_all | solution.py:91
Sparse Core Ops, SparseCore 0:
  47.2 51.4 all-gather.1
